TPU v7x, 32 devices: a whole 2x2x4 slice. The times are simulated.
32 devices in a mesh: rep: 2 (over x), fs: 4 (over z), tp: 4 (over y, core).
Axes of the slice: x: 2, y: 2, z: 4, core: 2. Of those that a mesh axis runs over, the one named last changes fastest.
Arguments:
- tokens: bfloat16 [4096, 2048], P(('rep', 'fs', 'tp')), may hold values from -6 to 6
- norm_gain: float32 [2048], replicated, may hold values from 0.1 to 1.9
- gate_weight: float32 [2048, 5632], P('fs', 'tp'), may hold values from -0.125 to 0.125
- gate_scale: float32 [5632], P('tp'), may hold values from 0.5 to 2
- up_weight: float32 [2048, 5632], P('fs', 'tp'), may hold values from -0.125 to 0.125
- up_scale: float32 [5632], P('tp'), may hold values from 0.5 to 2
- down_weight: float32 [5632, 2048], P('tp', 'fs'), may hold values from -0.078125 to 0.078125
- down_scale: float32 [2048], P('fs'), may hold values from 0.5 to 2
Outputs:
- mixed: bfloat16 [4096, 2048], P(('rep', 'fs', 'tp'))
All inputs are finite; a program needn't handle non-finite values.
Results may differ from a plain program's by a relative error of at most 0.014.
Values may be sent and summed in bfloat16 or wider, within the bound.
A program may use at most 64 MiB of HBM per device.

v0:
```python
import jax
import jax.numpy as jnp
from jax import lax
from jax.sharding import PartitionSpec as P


def shards(
    tokens, norm_gain, gate_weight, gate_scale, up_weight, up_scale, down_weight, down_scale
):
    n_rep = lax.axis_size("rep")
    rep = lax.axis_index("rep")
    width = gate_weight.shape[1] // n_rep
    start = rep * width

    def part(array, axis):
        return lax.dynamic_slice_in_dim(array, start, width, axis)

    flat = tokens.astype(jnp.float32)
    mean_square = jnp.mean(flat * flat, axis=-1, keepdims=True)
    inverse = lax.rsqrt(mean_square + 1e-06)
    normed = (flat * inverse * norm_gain).astype(jnp.bfloat16)
    group = lax.all_gather(normed, ("rep", "tp"), axis=0, tiled=True)
    gate_low = part(gate_weight, 1).astype(jnp.bfloat16)
    up_low = part(up_weight, 1).astype(jnp.bfloat16)
    down_low = part(down_weight, 0).astype(jnp.bfloat16)
    gate = jnp.dot(
        group,
        lax.all_gather(gate_low, "fs", axis=0, tiled=True),
        preferred_element_type=jnp.float32,
    )
    up = jnp.dot(
        group, lax.all_gather(up_low, "fs", axis=0, tiled=True), preferred_element_type=jnp.float32
    )
    down_full = lax.all_gather(down_low, "fs", axis=1, tiled=True)
    gate = gate * part(gate_scale, 0)
    up = up * part(up_scale, 0)
    hidden = (jax.nn.silu(gate) * up).astype(jnp.bfloat16)
    scales = lax.all_gather(down_scale, "fs", axis=0, tiled=True)
    total = lax.psum_scatter(
        jnp.dot(hidden, down_full, preferred_element_type=jnp.float32).astype(jnp.bfloat16),
        ("rep", "tp"),
        scatter_dimension=0,
        tiled=True,
    ).astype(jnp.float32)
    return (total * scales).astype(jnp.bfloat16)


def solution(mesh):
    in_specs = (
        P(("rep", "fs", "tp"), None),
        P(),
        P("fs", "tp"),
        P("tp"),
        P("fs", "tp"),
        P("tp"),
        P("tp", "fs"),
        P("fs"),
    )
    out_specs = P(("rep", "fs", "tp"), None)
    return jax.shard_map(shards, mesh=mesh, in_specs=in_specs, out_specs=out_specs, check_vma=False)
```

profile of v0, /device:TPU:0, one launch (start us, length us, event | category | flops | bytes accessed | tf_op | source)
XLA Modules:
  0.0 308.1 jit_solution(6207909742359432319)
XLA Ops:
  6.5 0.0 copy-start
  6.5 0.0 copy-start.1
  6.5 0.0 copy-start.2
  6.5 0.0 all-gather.8.cloned.1.call-start
  6.6 1.8 copy-done
  8.4 1.2 dynamic-slice_convert_fusion.1
  9.6 0.0 all-gather.8.cloned.1.call-update
  9.6 0.0 all-gather.6.cloned.1.call-start
  9.7 1.2 fusion
  10.9 0.0 copy-done.1
  10.9 0.0 copy-done.2
  10.9 0.0 copy-start.4
  10.9 0.0 copy-start.5
  10.9 1.0 fusion.2
  11.9 0.0 all-gather.6.cloned.1.call-update
  11.9 0.0 all-gather.10.cloned.1.call-start
  12.0 2.7 dynamic-slice_convert_fusion
  14.7 0.0 all-gather.10.cloned.1.call-update
  14.8 0.0 all-gather.12.cloned.1.call-start
  14.8 2.3 dynamic-slice_convert_fusion.2
  17.1 0.0 all-gather.12.cloned.1.call-update
  17.2 0.0 reduce-scatter.2.cloned.1.call-start
  17.2 0.0 copy-done.4
  17.2 0.1 dynamic_slice.16
  17.3 0.0 copy-done.5
  17.3 0.1 dynamic_slice.18
  17.4 58.6 %all-gather.8.cloned.1.call-done = bf16[2048,704]{1,0:T(8,128)(2,1)} async-done(((bf16[512,704]{1,0:T(8,128)(2,1)}), bf16[2048,704]{1,0:T(8,128)(2,1)}) %all-gather.8.cloned.1.call-update) | async-done | bytes 2883600 | tf_op jit(solution)/shard_map/all_gather | solution.py:28
  75.9 37.1 %all-gather.6.cloned.1.call-done = bf16[1024,2048]{1,0:T(8,128)(2,1)} async-done(((bf16[128,2048]{1,0:T(8,128)(2,1)}), bf16[1024,2048]{1,0:T(8,128)(2,1)}) %all-gather.6.cloned.1.call-update) | async-done | bytes 4194320 | tf_op jit(solution)/shard_map/all_gather | solution.py:22
  113.1 7.9 %fusion.4 = f32[1024,704]{0,1:T(8,128)} fusion(bf16[1024,2048]{1,0:T(8,128)(2,1)} %all-gather.6.cloned.1.call-done, bf16[2048,704]{1,0:T(8,128)(2,1)} %all-gather.8.cloned.1.call-done), kind=kOutput, calls=%fused_computation.13 | convolution fusion | flops 2952790016 | bytes 9961472 | tf_op jit(solution)/shard_map/dot_general | solution.py:26
  121.0 57.1 %all-gather.10.cloned.1.call-done = bf16[2048,704]{1,0:T(8,128)(2,1)} async-done(((bf16[512,704]{1,0:T(8,128)(2,1)}), bf16[2048,704]{1,0:T(8,128)(2,1)}) %all-gather.10.cloned.1.call-update) | async-done | bytes 2883600 | tf_op jit(solution)/shard_map/all_gather | solution.py:32
  178.1 59.2 %all-gather.12.cloned.1.call-done = bf16[704,2048]{1,0:T(8,128)(2,1)} async-done(((bf16[704,512]{1,0:T(8,128)(2,1)}), bf16[704,2048]{1,0:T(8,128)(2,1)}) %all-gather.12.cloned.1.call-update) | async-done | bytes 2883600 | tf_op jit(solution)/shard_map/all_gather | solution.py:34
  237.3 12.3 %convolution_convert_fusion = bf16[1024,2048]{1,0:T(8,128)(2,1)} fusion(bf16[704,2048]{1,0:T(8,128)(2,1)} %all-gather.12.cloned.1.call-done, f32[1024,704]{0,1:T(8,128)} %fusion.4, bf16[1024,2048]{1,0:T(8,128)(2,1)} %all-gather.6.cloned.1.call-done, bf16[2048,704]{1,0:T(8,128)(2,1)} %all-gather.10.cloned.1.call-done, f32[704]{0:T(1024)S(1)} %dynamic_slice.18, ...), kind=kOutput, calls=%fused_computation | convolution fusion | flops 5913444352 | bytes 17044992 | tf_op jit(solution)/shard_map/dot_general | solution.py:40
  249.7 0.0 copy-start.3
  249.7 0.0 reduce-scatter.2.cloned.1.call-update
  249.7 0.7 copy-done.3
  250.3 11.9 %all-gather = f32[4,1,512]{2,1,0:T(1,128)S(1)} all-gather(f32[1,1,512]{2,1,0:T(1,128)S(1)} %bitcast.8), channel_id=1, replica_groups=mesh['rep'=2,'fs'=4,'tp'=4] {'fs'}, dimensions={0}, use_global_device_ids=true | all-gather | bytes 10240 | tf_op jit(solution)/shard_map/all_gather | solution.py:38
  262.3 37.4 %reduce-scatter.2.cloned.1.call-done = bf16[128,2048]{1,0:T(8,128)(2,1)} async-done(((bf16[1024,2048]{1,0:T(8,128)(2,1)}), bf16[128,2048]{1,0:T(8,128)(2,1)}) %reduce-scatter.2.cloned.1.call-update) | async-done | bytes 524304 | tf_op jit(solution)/shard_map/reduce_scatter | solution.py:39
  299.7 1.9 multiply_convert_fusion.1
  (1 shorter events, 0.0 us)
Async XLA Ops:
  6.5 1.8 copy-start
  6.5 4.4 %copy-start.1 = (bf16[128,2048]{1,0:T(8,128)(2,1)S(1)}, bf16[128,2048]{1,0:T(8,128)(2,1)}, u32[]{:S(2)}) copy-start(bf16[128,2048]{1,0:T(8,128)(2,1)} %param.8) | copy-start | bytes 1572868
  6.5 4.4 %copy-start.2 = (f32[2048]{0:T(1024)S(1)}, f32[2048]{0:T(1024)}, u32[]{:S(2)}) copy-start(f32[2048]{0:T(1024)} %param.9) | copy-start | bytes 24580
  6.5 69.4 %all-gather.8.cloned.1.call-start = ((), (), s32[]{:S(2)}) async-start(), calls=%async_computation.2 | async-start | bytes 3932160 | tf_op jit(solution)/shard_map/all_gather | solution.py:28
  9.6 103.5 %all-gather.6.cloned.1.call-start = ((), (), s32[]{:S(2)}) async-start(), calls=%async_computation.1 | async-start | bytes 4718592 | tf_op jit(solution)/shard_map/all_gather | solution.py:22
  10.9 6.3 %copy-start.4 = (f32[1408]{0:T(1024)S(1)}, f32[1408]{0:T(1024)}, u32[]{:S(2)}) copy-start(f32[1408]{0:T(1024)} %param.11) | copy-start | bytes 16900
  10.9 6.4 %copy-start.5 = (f32[1408]{0:T(1024)S(1)}, f32[1408]{0:T(1024)}, u32[]{:S(2)}) copy-start(f32[1408]{0:T(1024)} %param.13) | copy-start | bytes 16900
  11.9 166.2 %all-gather.10.cloned.1.call-start = ((), (), s32[]{:S(2)}) async-start(), calls=%async_computation.3 | async-start | bytes 3932160 | tf_op jit(solution)/shard_map/all_gather | solution.py:32
  14.8 222.6 %all-gather.12.cloned.1.call-start = ((), (), s32[]{:S(2)}) async-start(), calls=%async_computation.4 | async-start | bytes 3604480 | tf_op jit(solution)/shard_map/all_gather | solution.py:34
  17.2 282.5 %reduce-scatter.2.cloned.1.call-start = ((), (), s32[]{:S(2)}) async-start(), calls=%async_computation.5 | async-start | bytes 4718592 | tf_op jit(solution)/shard_map/reduce_scatter | solution.py:39
  249.7 0.7 copy-start.3
Sparse Core Ops, SparseCore 0:
  9.7 66.1 all-gather.7
  77.8 35.2 all-gather.5
  114.7 63.4 all-gather.9
  179.6 57.7 all-gather.11
  249.8 49.8 reduce-scatter.1
where the time goes:
time: 308 us
  waiting for transfers between devices  250 us (81%)
  matrix products  20.2 us (7%)
  between operations  13.2 us (4%)
  blocking collectives  11.9 us (4%)
  local copies, waits for them, and re-layouts  8.92 us (3%)
  other arithmetic  4.16 us (1%)
    all_gather x1, waiting for transfers between devices, shards(): down_full = lax.all_gather(down_low, 'fs', axis=1, tiled=True)  59.2 us
    all_gather x1, waiting for transfers between devices, shards(): lax.all_gather(gate_low, 'fs', axis=0, tiled=True)  58.6 us
    all_gather x1, waiting for transfers between devices, shards(): lax.all_gather(up_low, 'fs', axis=0, tiled=True)  57.1 us
    reduce_scatter x1, waiting for transfers between devices, shards(): lax.psum_scatter(jnp.dot(hidden, down_full, preferred_element_type=jnp.fl...  37.4 us
    all_gather x1, waiting for transfers between devices, shards(): group = lax.all_gather(normed, ('rep', 'tp'), axis=0, tiled=True)  37.1 us
    dot_general x1, matrix products, shards(): jnp.dot(hidden, down_full, preferred_element_type=jnp.float32)  12.3 us
    all_gather x1, blocking collectives, shards(): scales = lax.all_gather(down_scale, 'fs', axis=0, tiled=True)  11.9 us
    dot_general x1, matrix products, shards(): jnp.dot(group, lax.all_gather(gate_low, 'fs', axis=0, tiled=True), prefer...  7.9 us
  transfers between devices with their start and end apart: 5, of which 5 were waited for; matrix products, arithmetic and copies ran while one was open for 5% of the time, Pallas kernels for 0%

commit v1 on v0

--- a/solution.py
+++ b/solution.py
@@ -31,7 +31,14 @@
     up = jnp.dot(
         group, lax.all_gather(up_low, "fs", axis=0, tiled=True), preferred_element_type=jnp.float32
     )
-    down_full = lax.all_gather(down_low, "fs", axis=1, tiled=True)
+    size = lax.axis_size("fs")
+    forward = [(i, (i + 1) % size) for i in range(size)]
+    parts = [down_low]
+    for far in range(1, size):
+        parts = [lax.ppermute(parts[0], "fs", forward), *parts]
+    result = jnp.concatenate(parts, axis=1)
+    turn = (lax.axis_index("fs") + 1) * parts[-1].shape[1]
+    down_full = jnp.roll(result, turn, axis=1)
     gate = gate * part(gate_scale, 0)
     up = up * part(up_scale, 0)
     hidden = (jax.nn.silu(gate) * up).astype(jnp.bfloat16)

time: 308 us -> 278 us (0.903)
  waiting for transfers between devices: 250 us -> 187 us
  starting transfers between devices: 0.17 us -> 17.7 us
  local copies, waits for them, and re-layouts: 8.92 us -> 22.5 us
    ppermute x0 -> x3, waiting for transfers between devices: none -> 86.1 us  [shards(): parts = [lax.ppermute(parts[0], 'fs', forward), *parts]]
    all_gather x1 -> x0, waiting for transfers between devices: 59.2 us -> none  [shards(): down_full = lax.all_gather(down_low, 'fs', axis=1, tiled=True)]
    all_gather x1, waiting for transfers between devices: 58.6 us -> 0.01 us  [shards(): lax.all_gather(gate_low, 'fs', axis=0, tiled=True)]
    all_gather x1, waiting for transfers between devices: 37.1 us -> 6.15 us  [shards(): group = lax.all_gather(normed, ('rep', 'tp'), axis=0, tiled=True)]
    ppermute x0 -> x3, starting transfers between devices: none -> 17.6 us  [shards(): parts = [lax.ppermute(parts[0], 'fs', forward), *parts]]
    unnamed x12 -> x21, local copies, waits for them, and re-layouts: 2.48 us -> 15.9 us
  transfers between devices with their start and end apart: 5 -> 7, of which waited for: 5 -> 6; matrix products, arithmetic and copies ran while one was open for 5% -> 10% of each run, Pallas kernels for 0% -> 0%
where the time goes in v1:
time: 278 us
  waiting for transfers between devices  187 us (67%)
  local copies, waits for them, and re-layouts  22.5 us (8%)
  matrix products  20.2 us (7%)
  starting transfers between devices  17.7 us (6%)
  between operations  13.2 us (5%)
  blocking collectives  11.9 us (4%)
  other arithmetic  5.2 us (2%)
    ppermute x3, waiting for transfers between devices, shards(): parts = [lax.ppermute(parts[0], 'fs', forward), *parts]  86.1 us
    all_gather x1, waiting for transfers between devices, shards(): lax.all_gather(up_low, 'fs', axis=0, tiled=True)  57.1 us
    reduce_scatter x1, waiting for transfers between devices, shards(): lax.psum_scatter(jnp.dot(hidden, down_full, preferred_element_type=jnp.fl...  37.4 us
    ppermute x3, starting transfers between devices, shards(): parts = [lax.ppermute(parts[0], 'fs', forward), *parts]  17.6 us
    unnamed x21, local copies, waits for them, and re-layouts  15.9 us
    dot_general x1, matrix products, shards(): jnp.dot(hidden, down_full, preferred_element_type=jnp.float32)  12.3 us
    all_gather x1, blocking collectives, shards(): scales = lax.all_gather(down_scale, 'fs', axis=0, tiled=True)  11.9 us
    dot_general x1, matrix products, shards(): jnp.dot(group, lax.all_gather(gate_low, 'fs', axis=0, tiled=True), prefer...  7.9 us
  transfers between devices with their start and end apart: 7, of which 6 were waited for; matrix products, arithmetic and copies ran while one was open for 10% of the time, Pallas kernels for 0%

profile of v1, /device:TPU:0, one launch (start us, length us, event | category | flops | bytes accessed | tf_op | source)
XLA Modules:
  0.0 277.6 jit_solution(2320724168191950796)
XLA Ops:
  6.5 0.0 copy-start
  6.5 0.0 copy-start.5
  6.5 0.0 copy-start.6
  6.5 0.0 all-gather.7.cloned.1.call-start
  6.6 1.8 copy-done
  8.4 1.2 dynamic-slice_convert_fusion.1
  9.6 0.0 all-gather.7.cloned.1.call-update
  9.6 0.0 all-gather.5.cloned.1.call-start
  9.6 1.2 fusion.1
  10.9 2.0 fusion.3
  12.9 0.0 all-gather.5.cloned.1.call-update
  12.9 0.0 all-gather.9.cloned.1.call-start
  13.0 2.7 dynamic-slice_convert_fusion
  15.7 0.0 all-gather.9.cloned.1.call-update
  15.7 0.0 reduce-scatter.2.cloned.1.call-start
  15.8 1.5 dynamic-slice_convert_fusion.2
  17.3 3.1 %collective-permute-start = (bf16[704,512]{1,0:T(8,128)(2,1)S(1)}, bf16[704,512]{1,0:T(8,128)(2,1)S(1)}, u32[]{:S(2)}, u32[]{:S(2)}) collective-permute-start(bf16[704,512]{1,0:T(8,128)(2,1)S(1)} %dynamic-slice_convert_fusion.2), channel_id=1, source_target_pairs={{0,4},{4,8},{8,12},{12,0},{1,5},{5,9},{9,13},{13,1},{2,6},{6,10},{... | collective-permute-start | bytes 2162696 | tf_op jit(solution)/shard_map/ppermute | solution.py:38
  20.4 32.6 %collective-permute-done = bf16[704,512]{1,0:T(8,128)(2,1)S(1)} collective-permute-done((bf16[704,512]{1,0:T(8,128)(2,1)S(1)}, bf16[704,512]{1,0:T(8,128)(2,1)S(1)}, u32[]{:S(2)}, u32[]{:S(2)}) %collective-permute-start) | collective-permute-done | bytes 720928 | tf_op jit(solution)/shard_map/ppermute | solution.py:38
  52.9 0.0 copy-start.1
  52.9 0.9 copy-done.1
  53.8 14.5 %collective-permute-start.1 = (bf16[704,512]{1,0:T(8,128)(2,1)S(1)}, bf16[704,512]{1,0:T(8,128)(2,1)}, u32[]{:S(2)}, u32[]{:S(2)}) collective-permute-start(bf16[704,512]{1,0:T(8,128)(2,1)S(1)} %collective-permute-done), channel_id=1, source_target_pairs={{0,4},{4,8},{8,12},{12,0},{1,5},{5,9},{9,13},{13,1},{2,6},{6,10},{... | collective-permute-start | bytes 2162696 | tf_op jit(solution)/shard_map/ppermute | solution.py:38
  68.4 35.3 %collective-permute-done.1 = bf16[704,512]{1,0:T(8,128)(2,1)} collective-permute-done((bf16[704,512]{1,0:T(8,128)(2,1)S(1)}, bf16[704,512]{1,0:T(8,128)(2,1)}, u32[]{:S(2)}, u32[]{:S(2)}) %collective-permute-start.1) | collective-permute-done | bytes 720928 | tf_op jit(solution)/shard_map/ppermute | solution.py:38
  103.7 0.0 collective-permute-start.2
  103.7 0.0 copy-done.5
  103.7 0.1 dynamic_slice.20
  103.8 0.0 copy-done.6
  103.8 0.1 dynamic_slice.22
  103.8 0.0 copy-start.3
  103.8 18.2 %collective-permute-done.2 = bf16[704,512]{1,0:T(8,128)(2,1)} collective-permute-done((bf16[704,512]{1,0:T(8,128)(2,1)}, bf16[704,512]{1,0:T(8,128)(2,1)}, u32[]{:S(2)}, u32[]{:S(2)}) %collective-permute-start.2) | collective-permute-done | bytes 720928 | tf_op jit(solution)/shard_map/ppermute | solution.py:38
  122.1 2.1 constant_dynamic-update-slice_fusion.7
  124.1 2.1 constant_dynamic-update-slice_fusion.6
  126.2 2.3 constant_dynamic-update-slice_fusion.5
  128.5 0.0 copy-done.3
  128.5 1.0 constant_dynamic-update-slice_fusion.4
  129.5 2.1 constant_dynamic-update-slice_fusion.3
  131.6 2.1 constant_dynamic-update-slice_fusion.2
  133.7 0.0 copy-done.2
  133.7 1.0 constant_dynamic-update-slice_fusion.1
  134.6 1.0 constant_dynamic-update-slice_fusion
  135.6 6.1 %all-gather.5.cloned.1.call-done = bf16[1024,2048]{1,0:T(8,128)(2,1)} async-done(((bf16[128,2048]{1,0:T(8,128)(2,1)}), bf16[1024,2048]{1,0:T(8,128)(2,1)}) %all-gather.5.cloned.1.call-update) | async-done | bytes 4194320 | tf_op jit(solution)/shard_map/all_gather | solution.py:22
  141.8 7.9 %fusion.6 = f32[1024,704]{0,1:T(8,128)} fusion(bf16[1024,2048]{1,0:T(8,128)(2,1)} %all-gather.5.cloned.1.call-done, bf16[2048,704]{1,0:T(8,128)(2,1)} %all-gather.7.cloned.1.call-done), kind=kOutput, calls=%fused_computation.23 | convolution fusion | flops 2952790016 | bytes 9961472 | tf_op jit(solution)/shard_map/dot_general | solution.py:26
  149.7 57.1 %all-gather.9.cloned.1.call-done = bf16[2048,704]{1,0:T(8,128)(2,1)} async-done(((bf16[512,704]{1,0:T(8,128)(2,1)}), bf16[2048,704]{1,0:T(8,128)(2,1)}) %all-gather.9.cloned.1.call-update) | async-done | bytes 2883600 | tf_op jit(solution)/shard_map/all_gather | solution.py:32
  206.8 12.3 %convolution_convert_fusion = bf16[1024,2048]{1,0:T(8,128)(2,1)} fusion(bf16[704,4096]{1,0:T(8,128)(2,1)} %constant_dynamic-update-slice_fusion, s32[]{:T(128)S(6)} %select_n.22, f32[1024,704]{0,1:T(8,128)} %fusion.6, bf16[1024,2048]{1,0:T(8,128)(2,1)} %all-gather.5.cloned.1.call-done, bf16[2048,704]{1,0:T(8,128)(2,1)} %all-gather.9.cloned.1.call-done, ...), kind=kOutput, calls=%fused_computation | convolution fusion | flops 5913444352 | bytes 17307140 | tf_op jit(solution)/shard_map/dot_general | solution.py:47
  219.1 0.0 reduce-scatter.2.cloned.1.call-update
  219.1 0.7 copy-done.4
  219.8 11.9 %all-gather = f32[4,1,512]{2,1,0:T(1,128)S(1)} all-gather(f32[1,1,512]{2,1,0:T(1,128)S(1)} %bitcast.7), channel_id=1, replica_groups=mesh['rep'=2,'fs'=4,'tp'=4] {'fs'}, dimensions={0}, use_global_device_ids=true | all-gather | bytes 10240 | tf_op jit(solution)/shard_map/all_gather | solution.py:45
  231.7 37.4 %reduce-scatter.2.cloned.1.call-done = bf16[128,2048]{1,0:T(8,128)(2,1)} async-done(((bf16[1024,2048]{1,0:T(8,128)(2,1)}), bf16[128,2048]{1,0:T(8,128)(2,1)}) %reduce-scatter.2.cloned.1.call-update) | async-done | bytes 524304 | tf_op jit(solution)/shard_map/reduce_scatter | solution.py:46
  269.1 1.9 multiply_convert_fusion.1
  (4 shorter events, 0.0 us)
Async XLA Ops:
  6.5 1.8 copy-start
  6.5 97.1 %copy-start.5 = (f32[1408]{0:T(1024)S(1)}, f32[1408]{0:T(1024)}, u32[]{:S(2)}) copy-start(f32[1408]{0:T(1024)} %param.11) | copy-start | bytes 16900
  6.5 97.2 %copy-start.6 = (f32[1408]{0:T(1024)S(1)}, f32[1408]{0:T(1024)}, u32[]{:S(2)}) copy-start(f32[1408]{0:T(1024)} %param.13) | copy-start | bytes 16900
  6.5 129.1 %all-gather.7.cloned.1.call-start = ((), (), s32[]{:S(2)}) async-start(), calls=%async_computation.2 | async-start | bytes 3932160 | tf_op jit(solution)/shard_map/all_gather | solution.py:28
  9.6 132.2 %all-gather.5.cloned.1.call-start = ((), (), s32[]{:S(2)}) async-start(), calls=%async_computation.1 | async-start | bytes 4718592 | tf_op jit(solution)/shard_map/all_gather | solution.py:22
  12.9 193.9 %all-gather.9.cloned.1.call-start = ((), (), s32[]{:S(2)}) async-start(), calls=%async_computation.3 | async-start | bytes 3932160 | tf_op jit(solution)/shard_map/all_gather | solution.py:32
  15.7 253.4 %reduce-scatter.2.cloned.1.call-start = ((), (), s32[]{:S(2)}) async-start(), calls=%async_computation.4 | async-start | bytes 4718592 | tf_op jit(solution)/shard_map/reduce_scatter | solution.py:46
  17.3 35.7 %collective-permute-start = (bf16[704,512]{1,0:T(8,128)(2,1)S(1)}, bf16[704,512]{1,0:T(8,128)(2,1)S(1)}, u32[]{:S(2)}, u32[]{:S(2)}) collective-permute-start(bf16[704,512]{1,0:T(8,128)(2,1)S(1)} %dynamic-slice_convert_fusion.2), channel_id=1, source_target_pairs={{0,4},{4,8},{8,12},{12,0},{1,5},{5,9},{9,13},{13,1},{2,6},{6,10},{... | collective-permute-start | bytes 2162696 | tf_op jit(solution)/shard_map/ppermute | solution.py:38
  52.9 0.9 copy-start.1
  53.8 49.8 %collective-permute-start.1 = (bf16[704,512]{1,0:T(8,128)(2,1)S(1)}, bf16[704,512]{1,0:T(8,128)(2,1)}, u32[]{:S(2)}, u32[]{:S(2)}) collective-permute-start(bf16[704,512]{1,0:T(8,128)(2,1)S(1)} %collective-permute-done), channel_id=1, source_target_pairs={{0,4},{4,8},{8,12},{12,0},{1,5},{5,9},{9,13},{13,1},{2,6},{6,10},{... | collective-permute-start | bytes 2162696 | tf_op jit(solution)/shard_map/ppermute | solution.py:38
  103.7 18.4 %collective-permute-start.2 = (bf16[704,512]{1,0:T(8,128)(2,1)}, bf16[704,512]{1,0:T(8,128)(2,1)}, u32[]{:S(2)}, u32[]{:S(2)}) collective-permute-start(bf16[704,512]{1,0:T(8,128)(2,1)} %collective-permute-done.1), channel_id=1, source_target_pairs={{0,4},{4,8},{8,12},{12,0},{1,5},{5,9},{9,13},{13,1},{2,6},{6,10},{... | collective-permute-start | bytes 2162696 | tf_op jit(solution)/shard_map/ppermute | solution.py:38
  103.8 24.6 %copy-start.3 = (f32[1408,512]{1,0:T(8,128)S(1)}, f32[1408,512]{1,0:T(8,128)}, u32[]{:S(2)}) copy-start(f32[1408,512]{1,0:T(8,128)} %param.14) | copy-start | bytes 8650756
  103.8 29.8 %copy-start.2 = (bf16[704,512]{1,0:T(8,128)(2,1)S(1)}, bf16[704,512]{1,0:T(8,128)(2,1)}, u32[]{:S(2)}) copy-start(bf16[704,512]{1,0:T(8,128)(2,1)} %copy-done.1) | copy-start | bytes 2162692
  219.1 0.7 copy-start.4
Sparse Core Ops, SparseCore 0:
  9.7 95.3 all-gather.6
  107.0 34.7 all-gather.4
  143.3 63.4 all-gather.8
  219.3 49.8 reduce-scatter.1
